TPU v7x, 32 devices: a whole 2x2x4 slice. The times are simulated.
32 devices in a mesh: sp: 8 (over z, x), tp: 4 (over y, core).
Axes of the slice: x: 2, y: 2, z: 4, core: 2. Of those that a mesh axis runs over, the one named last changes fastest.
Arguments:
- residual: bfloat16 [2048, 2048], P(('sp', 'tp')), may hold values from -6 to 6
- first_query: bfloat16 [2048, 512], P('sp', 'tp'), may hold values from -6 to 6
- second_query: bfloat16 [2048, 512], P('sp', 'tp'), may hold values from -6 to 6
- first_key: bfloat16 [2048, 512], P('sp', 'tp'), may hold values from -6 to 6
- second_key: bfloat16 [2048, 512], P('sp', 'tp'), may hold values from -6 to 6
- values: bfloat16 [2048, 1024], P('sp', 'tp'), may hold values from -6 to 6
- lambdas: float32 [8], P('tp'), may hold values from 0.3 to 0.8
- head_gain: float32 [128], replicated, may hold values from 0.1 to 1.9
- out_weight: bfloat16 [1024, 2048], P('tp'), may hold values from -0.1875 to 0.1875
- norm_gain: float32 [2048], replicated, may hold values from 0.1 to 1.9
- up_weight: bfloat16 [2048, 4096], P('sp', 'tp'), may hold values from -0.125 to 0.125
- down_weight: bfloat16 [4096, 2048], P('tp', 'sp'), may hold values from -0.09375 to 0.09375
Outputs:
- mixed: bfloat16 [2048, 2048], P(('sp', 'tp'))
All inputs are finite; a program needn't handle non-finite values.
Results may differ from a plain program's by a relative error of at most 0.019.
Values may be sent and summed in bfloat16 or wider, within the bound.
A program may use at most 128 MiB of HBM per device.

v0:
```python
import jax
import jax.numpy as jnp
from jax import lax
from jax.sharding import PartitionSpec as P


def rotate(blocked, positions):
    half = blocked.shape[-1] // 2
    inverse = 10000.0 ** (-jnp.arange(0, half, dtype=jnp.float32) * 2.0 / blocked.shape[-1])
    angle = positions[:, None] * inverse[None, :]
    cosine = jnp.cos(angle)[:, None, :]
    sine = jnp.sin(angle)[:, None, :]
    first, second = (blocked[..., :half], blocked[..., half:])
    return jnp.concatenate(
        [first * cosine - second * sine, second * cosine + first * sine], axis=-1
    )


def absorb(state, queries, keys, vals, factor):
    top, total, summed = state
    scores = jnp.einsum("qhe,khe->qhk", queries, keys, preferred_element_type=jnp.float32) * factor
    peak = jnp.maximum(top, jnp.max(scores, axis=-1))
    shrink = jnp.exp(top - peak)
    weights = jnp.exp(scores - peak[..., None])
    total = total * shrink + jnp.sum(weights, axis=-1)
    summed = summed * shrink[..., None] + jnp.einsum(
        "qhk,khe->qhe", weights.astype(jnp.bfloat16), vals, preferred_element_type=jnp.float32
    )
    return (peak, total, summed)


def layer_norm(stream, gain):
    center = stream - jnp.mean(stream, axis=-1, keepdims=True)
    spread = jnp.mean(center * center, axis=-1, keepdims=True)
    return center * lax.rsqrt(spread + 1e-05) * gain


def local(
    residual,
    first_query,
    second_query,
    first_key,
    second_key,
    values,
    lambdas,
    head_gain,
    out_weight,
    norm_gain,
    up_weight,
    down_weight,
):
    local_rows = first_query.shape[0]
    head_count = lambdas.shape[0]
    head_width = first_query.shape[1] // head_count
    value_width = values.shape[1] // head_count
    quarter_rows = local_rows // lax.axis_size("tp")
    factor = head_width ** (-0.5)
    positions = (lax.axis_index("sp") * local_rows + jnp.arange(local_rows)).astype(jnp.float32)

    def prepare(source):
        turned = rotate(
            source.astype(jnp.float32).reshape(local_rows, head_count, head_width), positions
        )
        return turned.astype(jnp.bfloat16)

    query_a, query_b = (prepare(first_query), prepare(second_query))
    key_a = prepare(first_key).reshape(local_rows, head_count * head_width)
    key_b = prepare(second_key).reshape(local_rows, head_count * head_width)
    start_state = (
        jnp.full((local_rows, head_count), -1e30, jnp.float32),
        jnp.zeros((local_rows, head_count), jnp.float32),
        jnp.zeros((local_rows, head_count, value_width), jnp.float32),
    )
    piece_a = lax.all_gather(key_a, "sp", axis=0, tiled=True)
    piece_b = lax.all_gather(key_b, "sp", axis=0, tiled=True)
    piece_v = lax.all_gather(values, "sp", axis=0, tiled=True)
    count = piece_a.shape[0]
    block = 512
    blocks = count // block

    def advance(state, item):
        block_a, block_b, block_v = item
        return (
            (
                absorb(state[0], query_a, block_a, block_v, factor),
                absorb(state[1], query_b, block_b, block_v, factor),
            ),
            None,
        )

    items = (
        piece_a.reshape(blocks, block, head_count, head_width),
        piece_b.reshape(blocks, block, head_count, head_width),
        piece_v.reshape(blocks, block, head_count, value_width),
    )
    state_a, state_b = lax.scan(advance, (start_state, start_state), items)[0]
    diff = state_a[2] / state_a[1][..., None] - lambdas[None, :, None] * (
        state_b[2] / state_b[1][..., None]
    )
    scale = lax.rsqrt(jnp.mean(diff * diff, axis=-1, keepdims=True) + 1e-05)
    flat = (
        (diff * scale * head_gain * 0.8)
        .astype(jnp.bfloat16)
        .reshape(local_rows, head_count * value_width)
    )
    projected = lax.psum(
        jnp.dot(flat, out_weight, preferred_element_type=jnp.float32).astype(jnp.bfloat16), "tp"
    ).astype(jnp.float32)
    stream = lax.all_gather(residual, "tp", axis=0, tiled=True)
    whole = layer_norm(stream.astype(jnp.float32) + projected, norm_gain).astype(jnp.bfloat16)
    own_normed = lax.dynamic_slice_in_dim(
        whole, lax.axis_index("tp") * quarter_rows, quarter_rows, 0
    )
    lifted = jnp.dot(
        whole,
        lax.all_gather(up_weight, "sp", axis=0, tiled=True),
        preferred_element_type=jnp.float32,
    )
    down_full = lax.all_gather(down_weight, "sp", axis=1, tiled=True)
    hidden = jnp.square(jax.nn.relu(lifted)).astype(jnp.bfloat16)
    lowered = lax.psum_scatter(
        jnp.dot(hidden, down_full, preferred_element_type=jnp.float32).astype(jnp.bfloat16),
        "tp",
        scatter_dimension=0,
        tiled=True,
    ).astype(jnp.float32)
    return (own_normed.astype(jnp.float32) + lowered).astype(jnp.bfloat16)


def solution(mesh):
    in_specs = (
        P(("sp", "tp"), None),
        P("sp", "tp"),
        P("sp", "tp"),
        P("sp", "tp"),
        P("sp", "tp"),
        P("sp", "tp"),
        P("tp"),
        P(),
        P("tp", None),
        P(),
        P("sp", "tp"),
        P("tp", "sp"),
    )
    out_specs = P(("sp", "tp"), None)
    return jax.shard_map(local, mesh=mesh, in_specs=in_specs, out_specs=out_specs, check_vma=False)
```

profile of v0, /device:TPU:0, one launch (start us, length us, event | category | flops | bytes accessed | tf_op | source)
XLA Modules:
  0.0 354.3 jit_solution(2607594345238030326)
XLA Ops:
  12.2 34.2 %all_gather.21 = bf16[2048,128]{0,1:T(8,128)(2,1)S(1)} all-gather(bf16[256,128]{0,1:T(8,128)(2,1)S(1)} %bitcast.66), channel_id=1, replica_groups=mesh['sp'=8,'tp'=4] {'sp'}, dimensions={0}, use_global_device_ids=true | all-gather | bytes 589824 | tf_op jit(solution)/shard_map/all_gather | solution.py:75
  47.7 31.6 %all_gather.19 = bf16[2048,128]{0,1:T(8,128)(2,1)S(1)} all-gather(bf16[256,128]{0,1:T(8,128)(2,1)S(1)} %bitcast.67), channel_id=1, replica_groups=mesh['sp'=8,'tp'=4] {'sp'}, dimensions={0}, use_global_device_ids=true | all-gather | bytes 589824 | tf_op jit(solution)/shard_map/all_gather | solution.py:74
  80.6 2.1 reshape.134
  82.7 42.6 %while.21 = (s32[]{:T(128)}, f32[256,2]{0,1:T(2,128)S(1)}, f32[256,2]{0,1:T(2,128)}, f32[256,2,128]{0,2,1:T(8,128)}, f32[256,2]{0,1:T(2,128)S(1)}, /*index=5*/f3...) while((s32[]{:T(128)}, f32[256,2]{0,1:T(2,128)S(1)}, ...), condition=%wide.region_5.6_spmd.clone, body=%wide.region_0.5_spmd.clone.sunk | while | flops 204870656 | bytes 9381043 | solution.py:96
  86.3 1.8 constant_dynamic-slice_fusion.2
  89.2 1.7 fusion.68
  94.9 1.3 fusion.66
  96.2 1.8 constant_dynamic-slice_fusion.2
  99.1 2.0 fusion.68
  101.1 2.0 fusion.67
  107.3 1.8 constant_dynamic-slice_fusion.2
  110.2 2.0 fusion.68
  112.2 2.0 fusion.67
  118.4 1.8 constant_dynamic-slice_fusion.2
  121.4 2.0 fusion.68
  123.4 2.0 fusion.67
  127.3 1.4 convolution_convert_fusion.1
  130.0 35.5 %all-reduce.2.cloned.1.call-done = bf16[256,2048]{1,0:T(8,128)(2,1)} async-done(((bf16[256,2048]{1,0:T(8,128)(2,1)}), bf16[256,2048]{1,0:T(8,128)(2,1)}) %all-reduce.2.cloned.1.call-update) | async-done | bytes 1048592 | tf_op jit(solution)/shard_map/psum | solution.py:106
  165.4 2.0 fusion.25
  168.5 74.0 %all-gather.11.cloned.1.call-done = bf16[1024,2048]{1,0:T(8,128)(2,1)} async-done(((bf16[1024,256]{1,0:T(8,128)(2,1)}), bf16[1024,2048]{1,0:T(8,128)(2,1)}) %all-gather.11.cloned.1.call-update) | async-done | bytes 4194320 | tf_op jit(solution)/shard_map/all_gather | solution.py:119
  242.5 73.0 %all-gather.9.cloned.1.call-done = bf16[2048,1024]{1,0:T(8,128)(2,1)} async-done(((bf16[256,1024]{1,0:T(8,128)(2,1)}), bf16[2048,1024]{1,0:T(8,128)(2,1)}) %all-gather.9.cloned.1.call-update) | async-done | bytes 4194320 | tf_op jit(solution)/shard_map/all_gather | solution.py:116
  315.5 6.8 %convolution_convert_fusion = bf16[256,2048]{1,0:T(8,128)(2,1)} fusion(bf16[1024,2048]{1,0:T(8,128)(2,1)} %all-gather.11.cloned.1.call-done, bf16[256,2048]{1,0:T(8,128)(2,1)S(1)} %multiply_convert_fusion, bf16[2048,1024]{1,0:T(8,128)(2,1)} %all-gather.9.cloned.1.call-done), kind=kOutput, calls=%fused_computation.37 | convolution fusion | flops 2148794368 | bytes 10485760 | tf_op jit(solution)/shard_map/dot_general | solution.py:122
  322.3 23.5 %reduce-scatter.2.cloned.1.call-done = bf16[64,2048]{1,0:T(8,128)(2,1)} async-done(((bf16[256,2048]{1,0:T(8,128)(2,1)}), bf16[64,2048]{1,0:T(8,128)(2,1)}) %reduce-scatter.2.cloned.1.call-update) | async-done | bytes 262160 | tf_op jit(solution)/shard_map/reduce_scatter | solution.py:121
  345.8 1.7 add_convert_fusion
  (98 shorter events, 32.5 us)
Async XLA Ops:
  6.5 120.7 %copy-start = (bf16[256,2048]{1,0:T(8,128)(2,1)S(1)}, bf16[256,2048]{1,0:T(8,128)(2,1)}, u32[]{:S(2)}) copy-start(bf16[256,2048]{1,0:T(8,128)(2,1)} %param.22) | copy-start | bytes 3145732
  6.5 74.1 %all-gather.7.cloned.1.call-start = ((), (), s32[]{:S(2)}) async-start(), calls=%async_computation.2 | async-start | bytes 1179648 | tf_op jit(solution)/shard_map/all_gather | solution.py:76
  7.3 122.7 %all-gather.5.cloned.1.call-start = ((), (), s32[]{:S(2)}) async-start(), calls=%async_computation.1 | async-start | bytes 1310720 | tf_op jit(solution)/shard_map/all_gather | solution.py:109
  8.0 157.4 %all-reduce.2.cloned.1.call-start = ((), (), s32[]{:S(2)}) async-start(), calls=%async_computation.3 | async-start | bytes 2097152 | tf_op jit(solution)/shard_map/psum | solution.py:106
  86.3 4.7 %copy-start.3 = (f32[256,2]{0,1:T(2,128)S(1)}, f32[256,2]{0,1:T(2,128)}, u32[]{:S(2)}) copy-start(f32[256,2]{0,1:T(2,128)} %get-tuple-element.265) | copy-start | bytes 6148 | tf_op jit(solution)/shard_map/while
  96.2 4.9 %copy-start.3 = (f32[256,2]{0,1:T(2,128)S(1)}, f32[256,2]{0,1:T(2,128)}, u32[]{:S(2)}) copy-start(f32[256,2]{0,1:T(2,128)} %get-tuple-element.265) | copy-start | bytes 6148 | tf_op jit(solution)/shard_map/while
  107.3 4.9 %copy-start.3 = (f32[256,2]{0,1:T(2,128)S(1)}, f32[256,2]{0,1:T(2,128)}, u32[]{:S(2)}) copy-start(f32[256,2]{0,1:T(2,128)} %get-tuple-element.265) | copy-start | bytes 6148 | tf_op jit(solution)/shard_map/while
  118.4 4.9 %copy-start.3 = (f32[256,2]{0,1:T(2,128)S(1)}, f32[256,2]{0,1:T(2,128)}, u32[]{:S(2)}) copy-start(f32[256,2]{0,1:T(2,128)} %get-tuple-element.265) | copy-start | bytes 6148 | tf_op jit(solution)/shard_map/while
  128.7 113.7 %all-gather.11.cloned.1.call-start = ((), (), s32[]{:S(2)}) async-start(), calls=%async_computation.5 | async-start | bytes 4718592 | tf_op jit(solution)/shard_map/all_gather | solution.py:119
  129.3 186.1 %all-gather.9.cloned.1.call-start = ((), (), s32[]{:S(2)}) async-start(), calls=%async_computation.4 | async-start | bytes 4718592 | tf_op jit(solution)/shard_map/all_gather | solution.py:116
  129.4 38.6 %copy-start.4 = (f32[2048]{0:T(1024)S(1)}, f32[2048]{0:T(1024)}, u32[]{:S(2)}) copy-start(f32[2048]{0:T(1024)} %param.23) | copy-start | bytes 24580
  129.9 215.9 %reduce-scatter.2.cloned.1.call-start = ((), (), s32[]{:S(2)}) async-start(), calls=%async_computation.6 | async-start | bytes 1310720 | tf_op jit(solution)/shard_map/reduce_scatter | solution.py:121
  130.0 37.5 %copy-start.1 = (bf16[256,2048]{1,0:T(8,128)(2,1)S(1)}, bf16[256,2048]{1,0:T(8,128)(2,1)}, u32[]{:S(2)}) copy-start(bf16[256,2048]{1,0:T(8,128)(2,1)} %all-gather.5.cloned.1.call-done) | copy-start | bytes 3145732
  165.4 2.0 copy-start.2
Sparse Core Ops, SparseCore 0:
  9.5 45.4 all-gather.6
  56.5 15.4 all-gather.4
  128.9 36.5 all-reduce.1
  167.3 75.0 all-gather.10
  244.4 70.9 all-gather.8
  322.4 23.2 reduce-scatter.1
where the time goes:
time: 355 us; the launch traced here: 354 us
  waiting for transfers between devices  208 us (59%)
  blocking collectives  65.8 us (19%)
  matrix products  33 us (9%)
  local copies, waits for them, and re-layouts  20.2 us (6%)
  between operations  13.7 us (4%)
  other arithmetic  12.9 us (4%)
    all_gather x1, waiting for transfers between devices, local(): down_full = lax.all_gather(down_weight, 'sp', axis=1, tiled=True)  74 us
    all_gather x1, waiting for transfers between devices, local(): lax.all_gather(up_weight, 'sp', axis=0, tiled=True)  73 us
    psum x1, waiting for transfers between devices, local(): lax.psum(jnp.dot(flat, out_weight, preferred_element_type=jnp.float32).as...  35.5 us
    all_gather x1, blocking collectives, local(): piece_b = lax.all_gather(key_b, 'sp', axis=0, tiled=True)  34.2 us
    all_gather x1, blocking collectives, local(): piece_a = lax.all_gather(key_a, 'sp', axis=0, tiled=True)  31.6 us
    reduce_scatter x1, waiting for transfers between devices, local(): lax.psum_scatter(jnp.dot(hidden, down_full, preferred_element_type=jnp.fl...  23.5 us
    dot_general x8, matrix products, absorb(): jnp.einsum('qhk,khe->qhe', weights.astype(jnp.bfloat16), vals, preferred_...  14.6 us
    dynamic_slice x8, local copies, waits for them, and re-layouts, local(): state_a, state_b = lax.scan(advance, (start_state, start_state), items)[0]  11.8 us
  transfers between devices with their start and end apart: 6, of which 4 were waited for; matrix products, arithmetic and copies ran while one was open for 16% of the time, Pallas kernels for 0%

commit v1 on v0

--- a/solution.py
+++ b/solution.py
@@ -116,7 +116,8 @@
         lax.all_gather(up_weight, "sp", axis=0, tiled=True),
         preferred_element_type=jnp.float32,
     )
-    down_full = lax.all_gather(down_weight, "sp", axis=1, tiled=True)
+    then = lax.all_gather(down_weight, "sp")
+    down_full = jnp.concatenate(then, axis=1)
     hidden = jnp.square(jax.nn.relu(lifted)).astype(jnp.bfloat16)
     lowered = lax.psum_scatter(
         jnp.dot(hidden, down_full, preferred_element_type=jnp.float32).astype(jnp.bfloat16),

time: 355 us -> 354 us (level)
  waiting for transfers between devices: 208 us -> 201 us
  local copies, waits for them, and re-layouts: 20.2 us -> 26.7 us
    reshape x0 -> x1, local copies, waits for them, and re-layouts: none -> 6.48 us  [local(): down_full = jnp.concatenate(then, axis=1)]
    all_gather x1, waiting for transfers between devices: 73 us -> 66.8 us  [local(): lax.all_gather(up_weight, 'sp', axis=0, tiled=True)]
  transfers between devices with their start and end apart: 6 -> 6, of which waited for: 4 -> 4; matrix products, arithmetic and copies ran while one was open for 16% -> 18% of each run, Pallas kernels for 0% -> 0%
where the time goes in v1:
time: 354 us; the launch traced here: 353 us
  waiting for transfers between devices  201 us (57%)
  blocking collectives  65.8 us (19%)
  matrix products  33 us (9%)
  local copies, waits for them, and re-layouts  26.7 us (8%)
  between operations  13.7 us (4%)
  other arithmetic  12.9 us (4%)
    all_gather x1, waiting for transfers between devices, local(): then = lax.all_gather(down_weight, 'sp')  72.2 us
    all_gather x1, waiting for transfers between devices, local(): lax.all_gather(up_weight, 'sp', axis=0, tiled=True)  66.8 us
    psum x1, waiting for transfers between devices, local(): lax.psum(jnp.dot(flat, out_weight, preferred_element_type=jnp.float32).as...  35.6 us
    all_gather x1, blocking collectives, local(): piece_a = lax.all_gather(key_a, 'sp', axis=0, tiled=True)  34.2 us
    all_gather x1, blocking collectives, local(): piece_b = lax.all_gather(key_b, 'sp', axis=0, tiled=True)  31.6 us
    reduce_scatter x1, waiting for transfers between devices, local(): lax.psum_scatter(jnp.dot(hidden, down_full, preferred_element_type=jnp.fl...  23.5 us
    dot_general x8, matrix products, absorb(): jnp.einsum('qhk,khe->qhe', weights.astype(jnp.bfloat16), vals, preferred_...  14.6 us
    dynamic_slice x8, local copies, waits for them, and re-layouts, local(): state_a, state_b = lax.scan(advance, (start_state, start_state), items)[0]  11.8 us
  transfers between devices with their start and end apart: 6, of which 4 were waited for; matrix products, arithmetic and copies ran while one was open for 18% of the time, Pallas kernels for 0%

profile of v1, /device:TPU:0, one launch (start us, length us, event | category | flops | bytes accessed | tf_op | source)
XLA Modules:
  0.0 353.1 jit_solution(6376753761988505863)
XLA Ops:
  12.2 34.2 %all_gather.22 = bf16[2048,128]{0,1:T(8,128)(2,1)S(1)} all-gather(bf16[256,128]{0,1:T(8,128)(2,1)S(1)} %bitcast.72), channel_id=1, replica_groups=mesh['sp'=8,'tp'=4] {'sp'}, dimensions={0}, use_global_device_ids=true | all-gather | bytes 589824 | tf_op jit(solution)/shard_map/all_gather | solution.py:74
  47.7 31.6 %all_gather.24 = bf16[2048,128]{0,1:T(8,128)(2,1)S(1)} all-gather(bf16[256,128]{0,1:T(8,128)(2,1)S(1)} %bitcast.73), channel_id=1, replica_groups=mesh['sp'=8,'tp'=4] {'sp'}, dimensions={0}, use_global_device_ids=true | all-gather | bytes 589824 | tf_op jit(solution)/shard_map/all_gather | solution.py:75
  80.6 2.1 reshape.140
  82.7 42.6 %while.21 = (s32[]{:T(128)}, f32[256,2]{0,1:T(2,128)S(1)}, f32[256,2]{0,1:T(2,128)}, f32[256,2,128]{0,2,1:T(8,128)}, f32[256,2]{0,1:T(2,128)S(1)}, /*index=5*/f3...) while((s32[]{:T(128)}, f32[256,2]{0,1:T(2,128)S(1)}, ...), condition=%wide.region_5.6_spmd.clone, body=%wide.region_0.5_spmd.clone.sunk | while | flops 204870656 | bytes 9381043 | solution.py:96
  86.3 1.8 constant_dynamic-slice_fusion.2
  89.2 1.7 fusion.68
  96.2 1.8 constant_dynamic-slice_fusion.2
  99.1 2.0 fusion.68
  101.1 2.0 fusion.67
  107.3 1.8 constant_dynamic-slice_fusion.2
  110.2 2.0 fusion.68
  112.2 2.0 fusion.67
  118.4 1.8 constant_dynamic-slice_fusion.2
  121.4 2.0 fusion.68
  123.4 2.0 fusion.67
  127.3 1.4 convolution_convert_fusion.1
  130.0 35.6 %all-reduce.2.cloned.1.call-done = bf16[256,2048]{1,0:T(8,128)(2,1)} async-done(((bf16[256,2048]{1,0:T(8,128)(2,1)}), bf16[256,2048]{1,0:T(8,128)(2,1)}) %all-reduce.2.cloned.1.call-update) | async-done | bytes 1048592 | tf_op jit(solution)/shard_map/psum | solution.py:106
  165.6 2.0 fusion.25
  168.6 72.2 %all-gather.12.cloned.1.call-done = bf16[8192,256]{1,0:T(8,128)(2,1)} async-done(((bf16[1024,256]{1,0:T(8,128)(2,1)}), bf16[8192,256]{1,0:T(8,128)(2,1)}) %all-gather.12.cloned.1.call-update) | async-done | bytes 4194320 | tf_op jit(solution)/shard_map/all_gather | solution.py:119
  240.9 6.5 %copy.37 = bf16[1024,8,256]{0,2,1:T(8,128)(2,1)} copy(bf16[1024,8,256]{2,0,1:T(8,128)(2,1)} %bitcast.65) | data formatting | bytes 8388608 | tf_op jit(solution)/shard_map/reshape | solution.py:120
  247.4 66.8 %all-gather.10.cloned.1.call-done = bf16[2048,1024]{1,0:T(8,128)(2,1)} async-done(((bf16[256,1024]{1,0:T(8,128)(2,1)}), bf16[2048,1024]{1,0:T(8,128)(2,1)}) %all-gather.10.cloned.1.call-update) | async-done | bytes 4194320 | tf_op jit(solution)/shard_map/all_gather | solution.py:116
  314.2 6.8 %convolution_convert_fusion = bf16[256,2048]{1,0:T(8,128)(2,1)} fusion(bf16[1024,2048]{0,1:T(8,128)(2,1)} %bitcast.66, bf16[256,2048]{1,0:T(8,128)(2,1)S(1)} %multiply_convert_fusion, bf16[2048,1024]{1,0:T(8,128)(2,1)} %all-gather.10.cloned.1.call-done), kind=kOutput, calls=%fused_computation.37 | convolution fusion | flops 2148794368 | bytes 10485760 | tf_op jit(solution)/shard_map/dot_general | solution.py:123
  321.0 23.5 %reduce-scatter.2.cloned.1.call-done = bf16[64,2048]{1,0:T(8,128)(2,1)} async-done(((bf16[256,2048]{1,0:T(8,128)(2,1)}), bf16[64,2048]{1,0:T(8,128)(2,1)}) %reduce-scatter.2.cloned.1.call-update) | async-done | bytes 262160 | tf_op jit(solution)/shard_map/reduce_scatter | solution.py:122
  344.5 1.7 add_convert_fusion
  (99 shorter events, 33.8 us)
Async XLA Ops:
  6.5 120.7 %copy-start = (bf16[256,2048]{1,0:T(8,128)(2,1)S(1)}, bf16[256,2048]{1,0:T(8,128)(2,1)}, u32[]{:S(2)}) copy-start(bf16[256,2048]{1,0:T(8,128)(2,1)} %param.22) | copy-start | bytes 3145732
  6.5 74.1 %all-gather.8.cloned.1.call-start = ((), (), s32[]{:S(2)}) async-start(), calls=%async_computation.2 | async-start | bytes 1179648 | tf_op jit(solution)/shard_map/all_gather | solution.py:76
  7.3 122.7 %all-gather.6.cloned.1.call-start = ((), (), s32[]{:S(2)}) async-start(), calls=%async_computation.1 | async-start | bytes 1310720 | tf_op jit(solution)/shard_map/all_gather | solution.py:109
  8.0 157.6 %all-reduce.2.cloned.1.call-start = ((), (), s32[]{:S(2)}) async-start(), calls=%async_computation.3 | async-start | bytes 2097152 | tf_op jit(solution)/shard_map/psum | solution.py:106
  86.3 4.7 %copy-start.3 = (f32[256,2]{0,1:T(2,128)S(1)}, f32[256,2]{0,1:T(2,128)}, u32[]{:S(2)}) copy-start(f32[256,2]{0,1:T(2,128)} %get-tuple-element.277) | copy-start | bytes 6148 | tf_op jit(solution)/shard_map/while
  96.2 4.9 %copy-start.3 = (f32[256,2]{0,1:T(2,128)S(1)}, f32[256,2]{0,1:T(2,128)}, u32[]{:S(2)}) copy-start(f32[256,2]{0,1:T(2,128)} %get-tuple-element.277) | copy-start | bytes 6148 | tf_op jit(solution)/shard_map/while
  107.3 4.9 %copy-start.3 = (f32[256,2]{0,1:T(2,128)S(1)}, f32[256,2]{0,1:T(2,128)}, u32[]{:S(2)}) copy-start(f32[256,2]{0,1:T(2,128)} %get-tuple-element.277) | copy-start | bytes 6148 | tf_op jit(solution)/shard_map/while
  118.4 4.9 %copy-start.3 = (f32[256,2]{0,1:T(2,128)S(1)}, f32[256,2]{0,1:T(2,128)}, u32[]{:S(2)}) copy-start(f32[256,2]{0,1:T(2,128)} %get-tuple-element.277) | copy-start | bytes 6148 | tf_op jit(solution)/shard_map/while
  128.7 112.1 %all-gather.12.cloned.1.call-start = ((), (), s32[]{:S(2)}) async-start(), calls=%async_computation.6 | async-start | bytes 4718592 | tf_op jit(solution)/shard_map/all_gather | solution.py:119
  129.3 184.9 %all-gather.10.cloned.1.call-start = ((), (), s32[]{:S(2)}) async-start(), calls=%async_computation.4 | async-start | bytes 4718592 | tf_op jit(solution)/shard_map/all_gather | solution.py:116
  129.4 38.8 %copy-start.4 = (f32[2048]{0:T(1024)S(1)}, f32[2048]{0:T(1024)}, u32[]{:S(2)}) copy-start(f32[2048]{0:T(1024)} %param.23) | copy-start | bytes 24580
  129.9 214.6 %reduce-scatter.2.cloned.1.call-start = ((), (), s32[]{:S(2)}) async-start(), calls=%async_computation.5 | async-start | bytes 1310720 | tf_op jit(solution)/shard_map/reduce_scatter | solution.py:122
  130.0 37.6 %copy-start.1 = (bf16[256,2048]{1,0:T(8,128)(2,1)S(1)}, bf16[256,2048]{1,0:T(8,128)(2,1)}, u32[]{:S(2)}) copy-start(bf16[256,2048]{1,0:T(8,128)(2,1)} %all-gather.6.cloned.1.call-done) | copy-start | bytes 3145732
  165.6 2.0 copy-start.2
Sparse Core Ops, SparseCore 0:
  9.5 45.4 all-gather.7
  56.5 15.4 all-gather.5
  128.9 36.7 all-reduce.1
  167.6 73.2 all-gather.11
  242.8 71.3 all-gather.9
  321.1 23.3 reduce-scatter.1
